TPU v7x, 32 devices: a whole 2x2x4 slice. The times are simulated.
32 devices in a mesh: sp: 16 (over z, y, x), tp: 2 (over core).
Axes of the slice: x: 2, y: 2, z: 4, core: 2. Of those that a mesh axis runs over, the one named last changes fastest.
Arguments:
- residual: bfloat16 [6144, 2048], P('sp'), may hold values from -6 to 6
- queries: bfloat16 [6144, 2048], P('sp', 'tp'), may hold values from -48 to 48
- keys: bfloat16 [6144, 2048], P('sp', 'tp'), may hold values from -48 to 48
- values: bfloat16 [6144, 2048], P('sp', 'tp'), may hold values from -6 to 6
- gate_cache: float32 [6144, 32], P('sp', 'tp'), may hold values from -1544 to 0, as said below
- doc_ids: int32 [6144], P('sp'), may hold values from 0 to 7, never falling along the last dimension, each value on 1 to 1536 neighbouring positions
- out_weight: bfloat16 [2048, 2048], P('tp'), may hold values from -1 to 1
- mix_gain: float32 [2048], replicated, may hold values from 0.1 to 1.9
- gate_weight: bfloat16 [2048, 5120], P('sp', 'tp'), may hold values from -0.125 to 0.125
- up_weight: bfloat16 [2048, 5120], P('sp', 'tp'), may hold values from -0.125 to 0.125
- down_weight: bfloat16 [5120, 2048], P('tp', 'sp'), may hold values from -0.15625 to 0.15625
Outputs:
- layer_out: bfloat16 [6144, 2048], P(('sp', 'tp'))
Inputs may be any that keep to these rules, and one draw needn't show every extreme that they name: `doc_ids`: positions of one document are consecutive; each document has 1 to 1536 positions, and one has exactly that many. `gate_cache`: no column rises from one position to the next.
All inputs are finite; a program needn't handle non-finite values.
Results may differ from a plain program's by a relative error of at most 0.018.
Values may be sent and summed in bfloat16 or wider, within the bound.
A program may use at most 128 MiB of HBM per device.

v0:
```python
import functools

import jax
import jax.numpy as jnp
from jax import lax
from jax.experimental import pallas as pl
from jax.experimental.pallas import tpu as pltpu
from jax.sharding import PartitionSpec as P

REACH = 4


EPSILON = 1e-06
NEGATIVE = -1e30


def from_behind(value, axis, steps):
    count = lax.axis_size(axis)
    first, last = (max(0, -steps), min(count, count - steps))
    return lax.ppermute(value, axis, [(source, source + steps) for source in range(first, last)])


def normalize(middle, gain):
    widened = middle.astype(jnp.float32)
    factor = lax.rsqrt(jnp.mean(widened * widened, axis=-1, keepdims=True) + EPSILON)
    return (widened * factor * gain).astype(jnp.bfloat16)


def plain_local(
    residual,
    queries,
    keys,
    values,
    gate_cache,
    doc_ids,
    out_weight,
    mix_gain,
    gate_weight,
    up_weight,
    down_weight,
):
    tok_rows = queries.shape[0]
    heads_here = gate_cache.shape[1]
    head_size = queries.shape[1] // heads_here
    sp_index = lax.axis_index("sp")
    key_parts = [keys]
    value_parts = [values]
    cache_parts = [gate_cache]
    doc_parts = [doc_ids]
    for distance in range(1, REACH + 1):
        moved_keys, moved_values = from_behind((keys, values), "sp", distance)
        moved_cache, moved_docs = from_behind((gate_cache, doc_ids), "sp", distance)
        key_parts.append(moved_keys)
        value_parts.append(moved_values)
        cache_parts.append(moved_cache)
        doc_parts.append(moved_docs)
    all_keys = jnp.concatenate(key_parts[::-1], axis=0)
    all_values = jnp.concatenate(value_parts[::-1], axis=0)
    all_cache = jnp.concatenate(cache_parts[::-1], axis=0)
    all_docs = jnp.concatenate(doc_parts[::-1], axis=0)
    key_count = all_keys.shape[0]
    query_pos = sp_index * tok_rows + jnp.arange(tok_rows, dtype=jnp.int32)
    key_pos = (sp_index - REACH) * tok_rows + jnp.arange(key_count, dtype=jnp.int32)
    visible = (
        (key_pos[None, :] <= query_pos[:, None])
        & (key_pos[None, :] >= 0)
        & (all_docs[None, :] == doc_ids[:, None])
    )
    query_heads = queries.reshape(tok_rows, heads_here, head_size)
    key_heads = all_keys.reshape(key_count, heads_here, head_size)
    value_heads = all_values.reshape(key_count, heads_here, head_size)
    score_scale = head_size ** (-0.5)
    scores = (
        jnp.einsum("qhd,khd->hqk", query_heads, key_heads, preferred_element_type=jnp.float32)
        * score_scale
    )
    scores = scores + gate_cache.T[:, :, None] - all_cache.T[:, None, :]
    scores = jnp.where(visible[None], scores, NEGATIVE)
    row_max = jnp.max(scores, axis=-1, keepdims=True)
    exp_scores = jnp.exp(scores - row_max)
    weights = (exp_scores / jnp.sum(exp_scores, axis=-1, keepdims=True)).astype(jnp.bfloat16)
    attended = jnp.einsum("hqk,khd->qhd", weights, value_heads, preferred_element_type=jnp.float32)
    attended = attended.astype(jnp.bfloat16).reshape(tok_rows, heads_here * head_size)
    row_share = tok_rows // lax.axis_size("tp")
    tp_index = lax.axis_index("tp")
    partial_value = jnp.dot(attended, out_weight, preferred_element_type=jnp.float32)
    attn_sum = lax.psum(partial_value.astype(jnp.bfloat16), "tp").astype(jnp.float32)
    whole_middle = (residual.astype(jnp.float32) + attn_sum).astype(jnp.bfloat16)
    mixer_in = normalize(whole_middle, mix_gain)
    middle = lax.dynamic_slice_in_dim(whole_middle, tp_index * row_share, row_share, 0)
    held_gate, held_up = (
        lax.all_gather(gate_weight, "sp", axis=0, tiled=True),
        lax.all_gather(up_weight, "sp", axis=0, tiled=True),
    )
    gate_proj = jnp.dot(mixer_in, held_gate, preferred_element_type=jnp.float32)
    up_proj = jnp.dot(mixer_in, held_up, preferred_element_type=jnp.float32)
    hidden = (jax.nn.silu(gate_proj) * up_proj).astype(jnp.bfloat16)
    partials = jnp.dot(
        hidden,
        lax.all_gather(down_weight, "sp", axis=1, tiled=True),
        preferred_element_type=jnp.float32,
    )
    down_sum = lax.psum_scatter(
        partials.astype(jnp.bfloat16), "tp", scatter_dimension=0, tiled=True
    ).astype(jnp.float32)
    return (middle.astype(jnp.float32) + down_sum).astype(jnp.bfloat16)


ROWS = 128


def attend_tile(tile, plane_index, span, head_size, queries, keys, values, aux, out):
    heads = queries.shape[1] // head_size
    q_start = pl.multiple_of(tile * ROWS, ROWS)
    window = span + ROWS
    key_aux = aux[:, pl.ds(q_start, window)]
    query_aux = jnp.transpose(aux[:, pl.ds(pl.multiple_of(q_start + span, ROWS), ROWS)])
    column = lax.broadcasted_iota(jnp.int32, (ROWS, window), 1)
    row = lax.broadcasted_iota(jnp.int32, (ROWS, window), 0)
    first = (1 - plane_index) * span - q_start
    visible = (
        (column <= row + span)
        & (column >= first)
        & (key_aux[heads : heads + 1, :] == query_aux[:, heads : heads + 1])
    )
    query = queries[pl.ds(q_start, ROWS), :] * jnp.bfloat16(head_size ** (-0.5))
    parts = []
    for head in range(heads):
        lanes = slice(head * head_size, (head + 1) * head_size)
        key = keys[pl.ds(q_start, window), lanes]
        scores = lax.dot_general(
            query[:, lanes], key, (((1,), (1,)), ((), ())), preferred_element_type=jnp.float32
        )
        scores = scores + (query_aux[:, head : head + 1] - key_aux[head : head + 1, :])
        scores = jnp.where(visible, scores, NEGATIVE)
        exp_scores = jnp.exp(scores - jnp.max(scores, axis=-1, keepdims=True))
        total = jnp.sum(exp_scores, axis=-1, keepdims=True)
        mixed = jnp.dot(
            exp_scores.astype(jnp.bfloat16),
            values[pl.ds(q_start, window), lanes],
            preferred_element_type=jnp.float32,
        )
        parts.append(mixed / total)
    out[pl.ds(q_start, ROWS), :] = jnp.concatenate(parts, axis=1).astype(jnp.bfloat16)


def attend_kernel(
    planes, group, head_size,
    queries, keys, values, aux, gate, up, down,
    attended, gate_all, up_all, down_all,
    q_buf, k_buf, v_buf, aux_buf, out_buf,
    a_send, a_recv, a_own, h_send, h_recv, w_send, w_recv, g_send, g_recv, w_own, b_send, b_recv, b_own,
):
    me = lax.axis_index("sp")
    plane, place = me // group, lax.rem(me, group)
    tok = queries.shape[0]
    cols = queries.shape[1] // group
    span = tok * group
    depth = gate.shape[0]
    width = gate.shape[1] // planes
    MESH = pl.DeviceIdType.MESH

    def neighbour(step):
        return lax.rem(place + step, group)

    def in_plane(step):
        return {"sp": plane * group + neighbour(step)}

    def other_plane(step):
        return lax.rem(plane + step, planes)

    def across(step):
        return {"sp": other_plane(step) * group + place}

    barrier = pltpu.get_barrier_semaphore()
    for step in range(1, group):
        pl.semaphore_signal(barrier, inc=1, device_id=in_plane(step), device_id_type=MESH)
    for step in range(1, planes):
        pl.semaphore_signal(barrier, inc=1, device_id=across(step), device_id_type=MESH)
    pl.semaphore_wait(barrier, group + planes - 2)

    def remote(src, dst, send, recv, device):
        return pltpu.make_async_remote_copy(
            src_ref=src, dst_ref=dst, send_sem=send, recv_sem=recv,
            device_id=device, device_id_type=MESH,
        )

    own_rows = pl.ds(pl.multiple_of(span + place * tok, 128), tok)
    q_rows = pl.ds(pl.multiple_of(place * tok, 128), tok)

    def head_cols(index):
        return pl.ds(pl.multiple_of(index * cols, 128), cols)

    spread = []
    for step in range(1, group):
        to = neighbour(step)
        for i, (src, dst, rows) in enumerate(
            ((keys, k_buf, own_rows), (values, v_buf, own_rows), (queries, q_buf, q_rows))
        ):
            spread.append(remote(src.at[:, head_cols(to)], dst.at[rows, :],
                                 a_send.at[i, step], a_recv.at[i, step], in_plane(step)))
        spread.append(remote(aux.at[to], aux_buf.at[:, own_rows],
                             a_send.at[3, step], a_recv.at[3, step], in_plane(step)))
    own = [
        pltpu.make_async_copy(keys.at[:, head_cols(place)], k_buf.at[own_rows, :], a_own.at[0]),
        pltpu.make_async_copy(values.at[:, head_cols(place)], v_buf.at[own_rows, :], a_own.at[1]),
        pltpu.make_async_copy(queries.at[:, head_cols(place)], q_buf.at[q_rows, :], a_own.at[2]),
        pltpu.make_async_copy(aux.at[place], aux_buf.at[:, own_rows], a_own.at[3]),
    ]
    for copy in spread + own:
        copy.start()

    def piece(m, part):
        at = pl.ds(pl.multiple_of(part * width, 128), width)
        return down.at[at, :] if m == 2 else (gate, up)[m].at[:, at]

    def slot(m, source_plane):
        at = pl.ds(pl.multiple_of((source_plane * group + place) * depth, 128), depth)
        return down_all.at[:, at] if m == 2 else (gate_all, up_all)[m].at[at, :]

    first = {
        (m, step): remote(piece(m, other_plane(step)), slot(m, plane),
                          w_send.at[m, step], w_recv.at[m, step], across(step))
        for m in range(3) for step in range(1, planes)
    }
    second = {}
    kept = [pltpu.make_async_copy(piece(m, plane), slot(m, plane), w_own.at[m]) for m in range(3)]
    for copy in kept:
        copy.start()

    def forward(m, source_step):
        source = lax.rem(plane + planes - source_step, planes)
        for step in range(1, group):
            src = piece(m, plane) if source_step == 0 else slot(m, source)
            copy = remote(src, slot(m, source), g_send.at[m, source_step, step],
                          g_recv.at[m, source_step, step], in_plane(step))
            copy.start()
            second[m, source_step, step] = copy

    for step in range(1, planes):
        first[0, step].start()
    for copy in own:
        copy.wait()
    for copy in spread:
        copy.wait()
    late, early = pl.ds(span, span), pl.ds(0, span)
    halo = [
        remote(k_buf.at[late, :], k_buf.at[early, :], h_send.at[0], h_recv.at[0], across(1)),
        remote(v_buf.at[late, :], v_buf.at[early, :], h_send.at[1], h_recv.at[1], across(1)),
        remote(aux_buf.at[:, late], aux_buf.at[:, early], h_send.at[2], h_recv.at[2], across(1)),
    ]
    for copy in halo:
        copy.start()
    for m in range(1, 3):
        for step in range(1, planes):
            first[m, step].start()
    for m in range(3):
        forward(m, 0)
    for m in range(3):
        for step in range(1, planes):
            first[m, step].wait()
            forward(m, step)
    for copy in halo:
        copy.wait()

    def one(tile, carry):
        attend_tile(tile, plane, span, head_size, q_buf, k_buf, v_buf, aux_buf, out_buf)
        return carry

    lax.fori_loop(0, span // ROWS, one, 0)

    back = []
    for step in range(1, group):
        rows = pl.ds(pl.multiple_of(neighbour(step) * tok, 128), tok)
        back.append(remote(out_buf.at[rows, :], attended.at[:, head_cols(place)],
                           b_send.at[step], b_recv.at[step], in_plane(step)))
    stay = pltpu.make_async_copy(out_buf.at[q_rows, :], attended.at[:, head_cols(place)], b_own)
    for copy in back:
        copy.start()
    stay.start()
    stay.wait()
    for copy in back + kept:
        copy.wait()
    for copy in second.values():
        copy.wait()


def attend_and_gather(queries, keys, values, aux, gate, up, down, planes, group, head_size):
    tok, all_cols = queries.shape
    cols, span = all_cols // group, tok * group
    features, width = gate.shape[0] * planes * group, gate.shape[1] // planes
    sem = pltpu.SemaphoreType.DMA
    anywhere = pl.BlockSpec(memory_space=pl.ANY)
    bf16 = jnp.bfloat16
    return pl.pallas_call(
        functools.partial(attend_kernel, planes, group, head_size),
        out_shape=(
            jax.ShapeDtypeStruct((tok, all_cols), bf16),
            jax.ShapeDtypeStruct((features, width), bf16),
            jax.ShapeDtypeStruct((features, width), bf16),
            jax.ShapeDtypeStruct((width, features), bf16),
        ),
        in_specs=[anywhere] * 7,
        out_specs=(anywhere,) * 4,
        scratch_shapes=[
            pltpu.VMEM((span, cols), bf16),
            pltpu.VMEM((2 * span, cols), bf16),
            pltpu.VMEM((2 * span, cols), bf16),
            pltpu.VMEM((8, 2 * span), jnp.float32),
            pltpu.VMEM((span, cols), bf16),
            sem((4, group)), sem((4, group)), sem((4,)),
            sem((3,)), sem((3,)),
            sem((3, planes)), sem((3, planes)),
            sem((3, planes, group)), sem((3, planes, group)),
            sem((3,)),
            sem((group,)), sem((group,)), sem,
        ],
        compiler_params=pltpu.CompilerParams(
            collective_id=0, has_side_effects=True, vmem_limit_bytes=40 * 1024 * 1024
        ),
    )(queries, keys, values, aux, gate, up, down)


def grouped_local(
    planes, group,
    residual, queries, keys, values, gate_cache, doc_ids,
    out_weight, mix_gain, gate_weight, up_weight, down_weight,
):
    tok_rows = queries.shape[0]
    heads_here = gate_cache.shape[1]
    head_size = queries.shape[1] // heads_here
    heads = heads_here // group
    rows = gate_cache.T.reshape(group, heads, tok_rows)
    docs = jnp.broadcast_to(doc_ids.astype(jnp.float32), (group, 1, tok_rows))
    fill = jnp.zeros((group, 7 - heads, tok_rows), jnp.float32)
    aux = jnp.concatenate([rows, docs, fill], axis=1)
    attended, gate, up, down = attend_and_gather(
        queries, keys, values, aux, gate_weight, up_weight, down_weight, planes, group, head_size
    )
    tp_count = lax.axis_size("tp")
    row_share = tok_rows // tp_count
    tp_index = lax.axis_index("tp")
    partial_value = jnp.dot(attended, out_weight, preferred_element_type=jnp.float32)
    return finish(
        planes, group, residual, partial_value.astype(jnp.bfloat16), mix_gain, gate, up, down,
        row_share, tp_index,
    )


def mix_kernel(
    planes, group,
    partial, residual, gain, gate, up, down, out,
    got, tokens, part, pair, sums, inbox, mid,
    x_send, x_recv, n_send, n_recv, z_send, z_recv, p_send, p_recv, r_send, r_recv,
):
    me, core = lax.axis_index("sp"), lax.axis_index("tp")
    plane, place = me // group, lax.rem(me, group)
    half, features = mid.shape
    other = 1 - core
    partner = {"tp": other}
    MESH = pl.DeviceIdType.MESH

    def across(step):
        return {"sp": lax.rem(plane + step, planes) * group + place}

    barrier = pltpu.get_barrier_semaphore()
    pl.semaphore_signal(barrier, inc=1, device_id=partner, device_id_type=MESH)
    for step in range(1, planes):
        pl.semaphore_signal(barrier, inc=1, device_id=across(step), device_id_type=MESH)
    pl.semaphore_wait(barrier, planes)

    def remote(src, dst, send, recv, device):
        copy = pltpu.make_async_remote_copy(
            src_ref=src, dst_ref=dst, send_sem=send, recv_sem=recv,
            device_id=device, device_id_type=MESH,
        )
        copy.start()
        return copy

    theirs = pl.ds(pl.multiple_of(other * half, 32), half)
    remote(partial.at[theirs, :], got, x_send, x_recv, partner).wait()
    chunk = 32

    def middle_rows(i, carry):
        at = pl.ds(pl.multiple_of(i * chunk, chunk), chunk)
        full = pl.ds(pl.multiple_of(core * half + i * chunk, chunk), chunk)
        total = partial[full, :].astype(jnp.float32) + got[at, :].astype(jnp.float32)
        middle = (residual[full, :].astype(jnp.float32) + total).astype(jnp.bfloat16)
        mid[at, :] = middle
        tokens[plane, core, at, :] = normalize(middle, gain[...])
        return carry

    lax.fori_loop(0, half // chunk, middle_rows, 0)
    mine = tokens.at[plane, core]
    near = [remote(mine, mine, n_send.at[0], n_recv.at[0], partner)]
    far = [None] + [
        remote(mine, mine, z_send.at[e], z_recv.at[e], across(e)) for e in range(1, planes)
    ]
    pairs, back = [], [None]
    for e in range(planes):
        source = lax.rem(plane + planes - e, planes)
        if e > 0:
            far[e].wait_recv()
            held = tokens.at[source, core]
            near.append(remote(held, held, n_send.at[e], n_recv.at[e], partner))
        near[e].wait_recv()
        block = tokens[source].reshape(2 * half, features)
        gate_proj = jnp.dot(block, gate[...], preferred_element_type=jnp.float32)
        up_proj = jnp.dot(block, up[...], preferred_element_type=jnp.float32)
        hidden = (gate_proj / (1.0 + jnp.exp(-gate_proj)) * up_proj).astype(jnp.bfloat16)
        lowered = jnp.dot(hidden, down[...], preferred_element_type=jnp.float32)
        part[source] = lowered.astype(jnp.bfloat16).reshape(2, half, features)
        pairs.append(remote(part.at[source, other], pair.at[source],
                            p_send.at[e], p_recv.at[e], partner))
        if e > 0:
            pairs[e].wait_recv()
            both = part[source, core].astype(jnp.float32) + pair[source].astype(jnp.float32)
            sums[source] = both.astype(jnp.bfloat16)
            back.append(remote(sums.at[source], inbox.at[e],
                               r_send.at[e], r_recv.at[e], across(planes - e)))
    pairs[0].wait_recv()
    for e in range(1, planes):
        back[e].wait_recv()

    def last_rows(i, carry):
        at = pl.ds(pl.multiple_of(i * chunk, chunk), chunk)
        total = part[plane, core, at, :].astype(jnp.float32)
        total = total + pair[plane, at, :].astype(jnp.float32)
        for e in range(1, planes):
            total = total + inbox[e, at, :].astype(jnp.float32)
        out[at, :] = (mid[at, :].astype(jnp.float32) + total).astype(jnp.bfloat16)
        return carry

    lax.fori_loop(0, half // chunk, last_rows, 0)
    for copy in near + far[1:] + pairs + back[1:]:
        copy.wait_send()


def finish(planes, group, residual, partial_value, mix_gain, gate, up, down, row_share, tp_index):
    features = residual.shape[1]
    sem = pltpu.SemaphoreType.DMA
    local_spec = pl.BlockSpec(memory_space=pltpu.VMEM)
    bf16 = jnp.bfloat16
    several = sem((planes,))
    return pl.pallas_call(
        functools.partial(mix_kernel, planes, group),
        out_shape=jax.ShapeDtypeStruct((row_share, features), bf16),
        in_specs=[local_spec] * 6,
        out_specs=local_spec,
        scratch_shapes=[
            pltpu.VMEM((row_share, features), bf16),
            pltpu.VMEM((planes, 2, row_share, features), bf16),
            pltpu.VMEM((planes, 2, row_share, features), bf16),
            pltpu.VMEM((planes, row_share, features), bf16),
            pltpu.VMEM((planes, row_share, features), bf16),
            pltpu.VMEM((planes, row_share, features), bf16),
            pltpu.VMEM((row_share, features), bf16),
            sem, sem, several, several, several, several, several, several, several, several,
        ],
        compiler_params=pltpu.CompilerParams(
            collective_id=1, has_side_effects=True, vmem_limit_bytes=58 * 1024 * 1024
        ),
    )(partial_value, residual, mix_gain.reshape(1, features), gate, up, down)


def choose(
    residual, queries, keys, values, gate_cache, doc_ids,
    out_weight, mix_gain, gate_weight, up_weight, down_weight,
):
    arrays = (
        residual, queries, keys, values, gate_cache, doc_ids,
        out_weight, mix_gain, gate_weight, up_weight, down_weight,
    )
    count, group = lax.axis_size("sp"), REACH
    planes = count // group
    heads = gate_cache.shape[1] // group
    fits = (
        count == planes * group
        and lax.axis_size("tp") == 2
        and queries.shape[0] % 64 == 0
        and gate_cache.shape[1] == heads * group
        and 1 <= heads <= 7
        and queries.shape[0] % 128 == 0
        and (queries.shape[1] // group) % 128 == 0
        and gate_weight.shape[0] % 128 == 0
        and gate_weight.shape[1] % (planes * 128) == 0
    )
    return grouped_local(planes, group, *arrays) if fits else plain_local(*arrays)


def solution(mesh):
    return jax.shard_map(
        choose,
        mesh=mesh,
        in_specs=(
            P("sp", None),
            P("sp", "tp"),
            P("sp", "tp"),
            P("sp", "tp"),
            P("sp", "tp"),
            P("sp"),
            P("tp", None),
            P(),
            P("sp", "tp"),
            P("sp", "tp"),
            P("tp", "sp"),
        ),
        out_specs=P(("sp", "tp"), None),
        check_vma=False,
    )
```

profile of v0, /device:TPU:0, one launch (start us, length us, event | category | flops | bytes accessed | tf_op | source)
XLA Modules:
  0.0 313.3 jit_solution(6663972897553650488)
XLA Ops:
  0.0 0.1 pad.2.clone
  0.1 0.7 convert_element_type.6
  0.8 0.7 reshape.6
  1.5 0.1 maximum_maximum_fusion.aux
  1.6 0.0 copy-start.3
  1.6 1.1 copy-done.3
  2.7 0.0 copy-start.4
  2.7 1.1 copy-done.4
  3.9 0.0 copy-start.5
  3.9 1.1 copy-done.5
  5.0 0.0 copy-start.6
  5.0 1.1 copy-done.6
  6.1 0.0 copy-start.7
  6.1 1.1 copy-done.7
  7.2 1.1 copy-done.8
  8.3 134.0 %shard_map.109 = (bf16[384,1024]{1,0:T(8,128)(2,1)S(1)}, bf16[2048,640]{1,0:T(8,128)(2,1)S(1)}, bf16[2048,640]{1,0:T(8,128)(2,1)S(1)}, bf16[640,2048]{1,0:T(8,128)(2,1)S(1)}) custom-call(bf16[384,1024]{1,0:T(8,128)(2,1)S(1)} %copy-done.3, bf16[384,1024]{1,0:T(8,128)(2,1)S(1)} %copy-done.4, bf16[384,1024]{1,0:T(8,128)(2,1)S(1)} %copy-done.5, ...), custom_call_target="tpu_custom_call" | custom-call | tf_op jit(solution)/shard_map/pallas_call | solution.py:295
  142.3 0.0 copy-start
  142.3 1.5 copy-done
  143.8 1.5 copy-done.1
  145.3 1.5 copy-done.2
  146.8 0.0 copy-done.9
  146.8 3.0 convolution_convert_fusion.partial
  149.9 161.3 %shard_map.110 = bf16[192,2048]{1,0:T(8,128)(2,1)} custom-call(bf16[384,2048]{1,0:T(8,128)(2,1)} %convolution_convert_fusion.partial, bf16[384,2048]{1,0:T(8,128)(2,1)} %residual.1, f32[1,2048]{1,0:T(1,128)} %bitcast.5, bf16[2048,640]{1,0:T(8,128)(2,1)} %copy-done, bf16[2048,640]{1,0:T(8,128)(2,1)} %copy-done.1, bf16[640,2048]{1,0:T(8,128)(2,1)} %copy-done.2), custom_call_target="tpu_custom_call" | custom-call | tf_op jit(solution)/shard_map/pallas_call | solution.py:445
  311.2 2.1 copy.13
  (6 shorter events, 0.0 us)
Async XLA Ops:
  1.6 1.1 copy-start.3
  2.7 1.1 copy-start.4
  3.9 1.1 copy-start.5
  5.0 1.1 copy-start.6
  6.1 1.1 copy-start.7
  7.2 1.1 copy-start.8
  8.3 138.6 %copy-start.9 = (bf16[1024,2048]{1,0:T(8,128)(2,1)S(1)}, bf16[1024,2048]{1,0:T(8,128)(2,1)}, u32[]{:S(2)}) copy-start(bf16[1024,2048]{1,0:T(8,128)(2,1)} %param.17) | copy-start | bytes 12582916
  142.3 1.5 copy-start
  143.8 1.5 copy-start.1
  145.3 1.5 copy-start.2
where the time goes:
time: 314 us; the launch traced here: 313 us
  Pallas kernels  295 us (94%)
  local copies, waits for them, and re-layouts  14.1 us (4%)
    pallas_call x1, Pallas kernels, finish(): pl.pallas_call(functools.partial(mix_kernel, planes, group), out_shape=ja...  161 us
    pallas_call x1, Pallas kernels, attend_and_gather(): pl.pallas_call(functools.partial(attend_kernel, planes, group, head_size)...  134 us
    unnamed x21, local copies, waits for them, and re-layouts  13.3 us

commit v1 on v0

v1 whole, which is shorter than its diff:
```python
import functools

import jax
import jax.numpy as jnp
from jax import lax
from jax.experimental import pallas as pl
from jax.experimental.pallas import tpu as pltpu
from jax.sharding import PartitionSpec as P

REACH = 4


EPSILON = 1e-06
NEGATIVE = -1e30


def from_behind(value, axis, steps):
    count = lax.axis_size(axis)
    first, last = (max(0, -steps), min(count, count - steps))
    return lax.ppermute(value, axis, [(source, source + steps) for source in range(first, last)])


def normalize(middle, gain):
    widened = middle.astype(jnp.float32)
    factor = lax.rsqrt(jnp.mean(widened * widened, axis=-1, keepdims=True) + EPSILON)
    return (widened * factor * gain).astype(jnp.bfloat16)


def plain_local(
    residual,
    queries,
    keys,
    values,
    gate_cache,
    doc_ids,
    out_weight,
    mix_gain,
    gate_weight,
    up_weight,
    down_weight,
):
    tok_rows = queries.shape[0]
    heads_here = gate_cache.shape[1]
    head_size = queries.shape[1] // heads_here
    sp_index = lax.axis_index("sp")
    key_parts = [keys]
    value_parts = [values]
    cache_parts = [gate_cache]
    doc_parts = [doc_ids]
    for distance in range(1, REACH + 1):
        moved_keys, moved_values = from_behind((keys, values), "sp", distance)
        moved_cache, moved_docs = from_behind((gate_cache, doc_ids), "sp", distance)
        key_parts.append(moved_keys)
        value_parts.append(moved_values)
        cache_parts.append(moved_cache)
        doc_parts.append(moved_docs)
    all_keys = jnp.concatenate(key_parts[::-1], axis=0)
    all_values = jnp.concatenate(value_parts[::-1], axis=0)
    all_cache = jnp.concatenate(cache_parts[::-1], axis=0)
    all_docs = jnp.concatenate(doc_parts[::-1], axis=0)
    key_count = all_keys.shape[0]
    query_pos = sp_index * tok_rows + jnp.arange(tok_rows, dtype=jnp.int32)
    key_pos = (sp_index - REACH) * tok_rows + jnp.arange(key_count, dtype=jnp.int32)
    visible = (
        (key_pos[None, :] <= query_pos[:, None])
        & (key_pos[None, :] >= 0)
        & (all_docs[None, :] == doc_ids[:, None])
    )
    query_heads = queries.reshape(tok_rows, heads_here, head_size)
    key_heads = all_keys.reshape(key_count, heads_here, head_size)
    value_heads = all_values.reshape(key_count, heads_here, head_size)
    score_scale = head_size ** (-0.5)
    scores = (
        jnp.einsum("qhd,khd->hqk", query_heads, key_heads, preferred_element_type=jnp.float32)
        * score_scale
    )
    scores = scores + gate_cache.T[:, :, None] - all_cache.T[:, None, :]
    scores = jnp.where(visible[None], scores, NEGATIVE)
    row_max = jnp.max(scores, axis=-1, keepdims=True)
    exp_scores = jnp.exp(scores - row_max)
    weights = (exp_scores / jnp.sum(exp_scores, axis=-1, keepdims=True)).astype(jnp.bfloat16)
    attended = jnp.einsum("hqk,khd->qhd", weights, value_heads, preferred_element_type=jnp.float32)
    attended = attended.astype(jnp.bfloat16).reshape(tok_rows, heads_here * head_size)
    row_share = tok_rows // lax.axis_size("tp")
    tp_index = lax.axis_index("tp")
    partial_value = jnp.dot(attended, out_weight, preferred_element_type=jnp.float32)
    attn_sum = lax.psum(partial_value.astype(jnp.bfloat16), "tp").astype(jnp.float32)
    whole_middle = (residual.astype(jnp.float32) + attn_sum).astype(jnp.bfloat16)
    mixer_in = normalize(whole_middle, mix_gain)
    middle = lax.dynamic_slice_in_dim(whole_middle, tp_index * row_share, row_share, 0)
    held_gate, held_up = (
        lax.all_gather(gate_weight, "sp", axis=0, tiled=True),
        lax.all_gather(up_weight, "sp", axis=0, tiled=True),
    )
    gate_proj = jnp.dot(mixer_in, held_gate, preferred_element_type=jnp.float32)
    up_proj = jnp.dot(mixer_in, held_up, preferred_element_type=jnp.float32)
    hidden = (jax.nn.silu(gate_proj) * up_proj).astype(jnp.bfloat16)
    partials = jnp.dot(
        hidden,
        lax.all_gather(down_weight, "sp", axis=1, tiled=True),
        preferred_element_type=jnp.float32,
    )
    down_sum = lax.psum_scatter(
        partials.astype(jnp.bfloat16), "tp", scatter_dimension=0, tiled=True
    ).astype(jnp.float32)
    return (middle.astype(jnp.float32) + down_sum).astype(jnp.bfloat16)


ROWS = 128


def attend_tile(tile, plane_index, span, head_size, queries, keys, values, aux, out):
    heads = queries.shape[1] // head_size
    q_start = pl.multiple_of(tile * ROWS, ROWS)
    window = span + ROWS
    key_aux = aux[:, pl.ds(q_start, window)]
    query_aux = jnp.transpose(aux[:, pl.ds(pl.multiple_of(q_start + span, ROWS), ROWS)])
    column = lax.broadcasted_iota(jnp.int32, (ROWS, window), 1)
    row = lax.broadcasted_iota(jnp.int32, (ROWS, window), 0)
    first = (1 - plane_index) * span - q_start
    visible = (
        (column <= row + span)
        & (column >= first)
        & (key_aux[heads : heads + 1, :] == query_aux[:, heads : heads + 1])
    )
    query = queries[pl.ds(q_start, ROWS), :] * jnp.bfloat16(head_size ** (-0.5))
    parts = []
    for head in range(heads):
        lanes = slice(head * head_size, (head + 1) * head_size)
        key = keys[pl.ds(q_start, window), lanes]
        scores = lax.dot_general(
            query[:, lanes], key, (((1,), (1,)), ((), ())), preferred_element_type=jnp.float32
        )
        scores = scores + (query_aux[:, head : head + 1] - key_aux[head : head + 1, :])
        scores = jnp.where(visible, scores, NEGATIVE)
        exp_scores = jnp.exp(scores - jnp.max(scores, axis=-1, keepdims=True))
        total = jnp.sum(exp_scores, axis=-1, keepdims=True)
        mixed = jnp.dot(
            exp_scores.astype(jnp.bfloat16),
            values[pl.ds(q_start, window), lanes],
            preferred_element_type=jnp.float32,
        )
        parts.append(mixed / total)
    out[pl.ds(q_start, ROWS), :] = jnp.concatenate(parts, axis=1).astype(jnp.bfloat16)


def layer_kernel(
    planes, head_size,
    residual, queries, keys, values, aux, out_weight, gain, gate, up, down,
    out,
    q_buf, k_buf, v_buf, aux_buf, out_buf, attended, out_w, res_buf,
    gate_all, up_all, down_all, theirs_buf, mine_buf, got, mid, tokens, hidden,
    part, pair, sums, inbox,
    a_send, a_recv, a_own, h_send, h_recv, w_send, w_recv, w_own, g_send, g_recv,
    b_send, b_recv, b_own, l_own, x_send, x_recv, n_send, n_recv, f_send, f_recv,
    p_send, p_recv, r_send, r_recv,
):
    group = REACH
    me, core = lax.axis_index("sp"), lax.axis_index("tp")
    plane, place = me // group, lax.rem(me, group)
    x, y = lax.rem(place, 2), place // 2
    low, high = lax.rem(plane, 2), plane // 2
    tok = queries.shape[0]
    cols = queries.shape[1] // group
    span = tok * group
    depth = gate.shape[0]
    width = gate.shape[1] // group
    half, features = mid.shape
    sources = 2 * planes
    MESH = pl.DeviceIdType.MESH
    other = 1 - core
    partner = {"tp": other}

    def turned(step):
        return lax.rem(x + lax.rem(step, 2), 2) + 2 * lax.rem(y + step // 2, 2)

    def in_plane(step):
        return {"sp": plane * group + turned(step)}

    def same_y(at_plane, at_x):
        return at_plane * group + 2 * y + at_x

    def target(e):
        return lax.rem(plane + e // 2, planes), lax.rem(x + e % 2, 2)

    y_neighbour = {"sp": plane * group + 2 * (1 - y) + x}
    above = {"sp": lax.rem(plane + 1, planes) * group + place}
    below = {"sp": lax.rem(plane + planes - 1, planes) * group + place}

    def member(e):
        return lax.rem(low + e // 2, 2), lax.rem(x + e % 2, 2)

    def quad(e):
        its_low, its_x = member(e)
        return {"sp": same_y(high * 2 + its_low, its_x)}

    def block(e):
        its_low, its_x = member(e)
        return its_low * 2 + its_x

    barrier = pltpu.get_barrier_semaphore()

    def greet(device):
        pl.semaphore_signal(barrier, inc=1, device_id=device, device_id_type=MESH)

    greet(partner)
    for step in range(2, group):
        greet(in_plane(step))
    for e in range(1, sources):
        greet({"sp": same_y(*target(e))})
    pl.semaphore_wait(barrier, group - 2 + sources)

    def remote(src, dst, send, recv, device):
        return pltpu.make_async_remote_copy(
            src_ref=src, dst_ref=dst, send_sem=send, recv_sem=recv,
            device_id=device, device_id_type=MESH,
        )

    def late(at_place):
        return pl.ds(pl.multiple_of(span + at_place * tok, 128), tok)

    def early(at_place):
        return pl.ds(pl.multiple_of(at_place * tok, 128), tok)

    def head_cols(index):
        return pl.ds(pl.multiple_of(index * cols, 128), cols)

    def spread(step, kinds):
        to = turned(step)
        every = (
            (keys.at[:, head_cols(to)], k_buf.at[late(place), :]),
            (values.at[:, head_cols(to)], v_buf.at[late(place), :]),
            (aux.at[to], aux_buf.at[:, late(place)]),
            (queries.at[:, head_cols(to)], q_buf.at[early(place), :]),
        )
        return [
            remote(*every[i], a_send.at[i, step], a_recv.at[i, step], in_plane(step))
            for i in kinds
        ]

    def halo(step):
        at = turned(step)
        every = (
            (k_buf.at[late(at), :], k_buf.at[early(at), :]),
            (v_buf.at[late(at), :], v_buf.at[early(at), :]),
            (aux_buf.at[:, late(at)], aux_buf.at[:, early(at)]),
        )
        if step == 0:
            own_src = (keys.at[:, head_cols(place)], values.at[:, head_cols(place)], aux.at[place])
            every = tuple((src, dst) for src, (_, dst) in zip(own_src, every))
        return [
            remote(*every[i], h_send.at[i, step], h_recv.at[i, step], above) for i in range(3)
        ]

    def halo_arrived(at):
        step = lax.rem(x + lax.rem(at, 2), 2) + 2 * lax.rem(y + at // 2, 2)
        for i, ref in enumerate((k_buf.at[early(at), :], v_buf.at[early(at), :], aux_buf.at[:, early(at)])):
            remote(ref, ref, h_send.at[i, step], h_recv.at[i, step], below).wait_recv()

    def piece(m, part_index):
        at = pl.ds(pl.multiple_of(part_index * width, 128), width)
        return down.at[at, :] if m == 2 else (gate, up)[m].at[:, at]

    def slot(m, source):
        at = pl.ds(pl.multiple_of(source * depth, 128), depth)
        return down_all.at[:, at] if m == 2 else (gate_all, up_all)[m].at[at, :]

    def weight(m, e):
        to_plane, to_x = target(e)
        index = lax.rem(to_plane, 2) * 2 + to_x
        return remote(piece(m, index), slot(m, me), w_send.at[m, e], w_recv.at[m, e],
                      {"sp": same_y(to_plane, to_x)})

    own_block = block(0)
    forward_own = [
        remote(piece(m, own_block), slot(m, me), g_send.at[m, 0], g_recv.at[m, 0], y_neighbour)
        for m in range(3)
    ]

    def pass_on(m, k):
        its_plane, dx = planes - 1 - k // 2, lax.rem(k, 2)
        e = lax.rem(plane - its_plane + planes, planes) * 2 + dx

        @pl.when(e != 0)
        def _():
            held = slot(m, same_y(its_plane, lax.rem(x + dx, 2)))
            remote(held, held, w_send.at[m, e], w_recv.at[m, e], y_neighbour).wait_recv()
            remote(held, held, g_send.at[m, e], g_recv.at[m, e], y_neighbour).start()

    def pass_range(m, first, last):
        def one(k, carry):
            pass_on(m, k)
            return carry

        lax.fori_loop(first, last, one, 0)

    def gathered(m):
        def one(e, carry):
            its_plane = lax.rem(plane - e // 2 + planes, planes)
            its_x = lax.rem(x + lax.rem(e, 2), 2)
            held = slot(m, its_plane * group + 2 * (1 - y) + its_x)
            remote(held, held, g_send.at[m, e], g_recv.at[m, e], y_neighbour).wait_recv()
            return carry

        lax.fori_loop(0, sources, one, 0)

    own = [
        pltpu.make_async_copy(keys.at[:, head_cols(place)], k_buf.at[late(place), :], a_own.at[0]),
        pltpu.make_async_copy(values.at[:, head_cols(place)], v_buf.at[late(place), :], a_own.at[1]),
        pltpu.make_async_copy(aux.at[place], aux_buf.at[:, late(place)], a_own.at[2]),
        pltpu.make_async_copy(queries.at[:, head_cols(place)], q_buf.at[early(place), :], a_own.at[3]),
    ]
    kept = [
        pltpu.make_async_copy(piece(m, own_block), slot(m, me), w_own.at[m]) for m in range(3)
    ]
    core_rows = pl.ds(pl.multiple_of(core * half, 64), half)
    loads = [
        pltpu.make_async_copy(out_weight, out_w, l_own.at[0]),
        pltpu.make_async_copy(residual.at[core_rows, :], res_buf, l_own.at[1]),
    ]
    has_above, has_below = plane < planes - 1, plane > 0

    first_kinds = {step: spread(step, (0, 1, 2)) for step in range(1, group)}
    query_kinds = {step: spread(step, (3,)) for step in range(1, group)}
    halos = {step: halo(step) for step in range(group)}
    for step in range(1, group):
        for copy in first_kinds[step]:
            copy.start()

    @pl.when(has_above)
    def _():
        for copy in halos[0]:
            copy.start()

    for step in range(1, group):
        for copy in query_kinds[step]:
            copy.start()
    for copy in own + kept + loads:
        copy.start()
    weights = {(m, e): weight(m, e) for m in range(3) for e in range(1, sources)}

    def upward(e):
        return jnp.logical_and(e // 2 > 0, plane + e // 2 < planes)

    for m in range(3):
        forward_own[m].start()
        for e in range(1, sources):
            pl.when(jnp.logical_not(upward(e)))(weights[m, e].start)

    @pl.when(plane == 0)
    def _():
        k_buf[pl.ds(0, span), :] = jnp.zeros((span, cols), jnp.bfloat16)
        v_buf[pl.ds(0, span), :] = jnp.zeros((span, cols), jnp.bfloat16)
        aux_buf[:, pl.ds(0, span)] = jnp.zeros((aux_buf.shape[0], span), jnp.float32)

    for step in range(1, group):
        for copy in first_kinds[step]:
            copy.wait_recv()

        @pl.when(has_above)
        def _():
            for copy in halos[step]:
                copy.start()

    for m in range(3):
        for e in range(2, sources):
            pl.when(upward(e))(weights[m, e].start)
    for step in range(1, group):
        for copy in query_kinds[step]:
            copy.wait_recv()
    for copy in own:
        copy.wait()

    def back(at, start):
        step = lax.rem(x + lax.rem(at, 2), 2) + 2 * lax.rem(y + at // 2, 2)
        rows = out_buf.at[early(at), :]

        @pl.when(at != place)
        def _():
            copy = remote(rows, attended.at[:, head_cols(place)], b_send.at[step], b_recv.at[step],
                          {"sp": plane * group + at})
            copy.start() if start else copy.wait_send()

        @pl.when(at == place)
        def _():
            copy = pltpu.make_async_copy(rows, attended.at[:, head_cols(place)], b_own)
            copy.start() if start else copy.wait()

    tiles = tok // ROWS
    skip = max(0, group * tiles - sources - 1)

    def rows_of(i, carry):
        at = group - 1 - i

        @pl.when(has_below)
        def _():
            halo_arrived(at)

        def one(j, inner):
            attend_tile(at * tiles + tiles - 1 - j, plane, span, head_size,
                        q_buf, k_buf, v_buf, aux_buf, out_buf)
            k = i * tiles + j - skip

            @pl.when(jnp.logical_and(k >= 0, k < sources))
            def _():
                pass_on(0, k)

            return inner

        lax.fori_loop(0, tiles, one, 0)
        back(at, True)
        return carry

    lax.fori_loop(0, group, rows_of, 0)
    pass_range(1, 0, planes)
    for step in range(1, group):
        its = attended.at[:, head_cols(turned(step))]
        remote(its, its, b_send.at[step], b_recv.at[step], in_plane(step)).wait_recv()
    back(place, False)
    for copy in loads:
        copy.wait()

    wide = 512

    def project(first_row, dst):
        def one(i, carry):
            at = pl.ds(pl.multiple_of(i * wide, wide), wide)
            dst[:, at] = jnp.dot(
                attended[pl.ds(pl.multiple_of(first_row, 64), half), :], out_w[:, at],
                preferred_element_type=jnp.float32,
            ).astype(jnp.bfloat16)
            return carry

        lax.fori_loop(0, features // wide, one, 0)

    project(other * half, theirs_buf)
    swap = remote(theirs_buf, got, x_send, x_recv, partner)
    swap.start()
    project(core * half, mine_buf)
    swap.wait_recv()
    chunk = 32

    def middle_rows(i, carry):
        at = pl.ds(pl.multiple_of(i * chunk, chunk), chunk)
        total = mine_buf[at, :].astype(jnp.float32) + got[at, :].astype(jnp.float32)
        middle = (res_buf[at, :].astype(jnp.float32) + total).astype(jnp.bfloat16)
        mid[at, :] = middle
        tokens[own_block, core, at, :] = normalize(middle, gain[...])
        return carry

    lax.fori_loop(0, half // chunk, middle_rows, 0)
    mine = tokens.at[own_block, core]
    far = {e: remote(mine, mine, f_send.at[e], f_recv.at[e], quad(e)) for e in range(1, group)}
    for e in (3, 1, 2):
        far[e].start()
    near = {}
    for e in range(group):
        held = tokens.at[block(e), core]
        near[e] = remote(held, held, n_send.at[e], n_recv.at[e], partner)
    near[0].start()
    pass_range(1, planes, sources)
    for e in range(1, group):
        far[e].wait_recv()
        near[e].start()
    for m in range(2):
        kept[m].wait()
        gathered(m)
    each = sources // group

    def gate_and_up(e, carry):
        index = lax.rem(low + e // 2, 2) * 2 + lax.rem(x + lax.rem(e, 2), 2)
        theirs = tokens.at[index, other]
        remote(theirs, theirs, n_send.at[e], n_recv.at[e], partner).wait_recv()
        rows = tokens[index].reshape(2 * half, features)
        gate_proj = jnp.dot(rows, gate_all[...], preferred_element_type=jnp.float32)
        up_proj = jnp.dot(rows, up_all[...], preferred_element_type=jnp.float32)
        hidden[index] = (gate_proj / (1.0 + jnp.exp(-gate_proj)) * up_proj).astype(jnp.bfloat16)
        pass_range(2, e * each, (e + 1) * each)
        return carry

    lax.fori_loop(0, group, gate_and_up, 0)
    kept[2].wait()
    gathered(2)
    order = (3, 1, 2, 0)
    pairs, sent = {}, {}

    def give(e):
        index = block(e)
        pairs[e].wait_recv()

        def one(i, carry):
            at = pl.ds(pl.multiple_of(i * chunk, chunk), chunk)
            both = part[index, core, at, :].astype(jnp.float32) + pair[index, at, :].astype(jnp.float32)
            sums[e, at, :] = both.astype(jnp.bfloat16)
            return carry

        lax.fori_loop(0, half // chunk, one, 0)
        sent[e] = remote(sums.at[e], inbox.at[e], r_send.at[e], r_recv.at[e], quad(e))
        sent[e].start()

    for i, e in enumerate(order):
        index = block(e)
        lowered = jnp.dot(hidden[index], down_all[...], preferred_element_type=jnp.float32)
        part[index] = lowered.astype(jnp.bfloat16).reshape(2, half, features)
        pairs[e] = remote(part.at[index, other], pair.at[index], p_send.at[e], p_recv.at[e], partner)
        pairs[e].start()
        if i > 0:
            give(order[i - 1])
    pairs[0].wait_recv()
    for e in range(1, group):
        sent[e].wait_recv()

    def last_rows(i, carry):
        at = pl.ds(pl.multiple_of(i * chunk, chunk), chunk)
        total = part[own_block, core, at, :].astype(jnp.float32)
        total = total + pair[own_block, at, :].astype(jnp.float32)
        for e in range(1, group):
            total = total + inbox[e, at, :].astype(jnp.float32)
        out[at, :] = (mid[at, :].astype(jnp.float32) + total).astype(jnp.bfloat16)
        return carry

    lax.fori_loop(0, half // chunk, last_rows, 0)

    for step in range(1, group):
        for copy in first_kinds[step] + query_kinds[step]:
            copy.wait_send()
        back(turned(step), False)

    @pl.when(has_above)
    def _():
        for step in range(group):
            for copy in halos[step]:
                copy.wait_send()

    for copy in list(weights.values()) + [swap] + list(far.values()) + list(near.values()):
        copy.wait_send()
    for copy in list(pairs.values()) + list(sent.values()):
        copy.wait_send()

    def drain(e, carry):
        for m in range(3):
            held = slot(m, me)
            remote(held, held, g_send.at[m, e], g_recv.at[m, e], y_neighbour).wait_send()
        return carry

    lax.fori_loop(0, sources, drain, 0)


def grouped_local(
    planes,
    residual, queries, keys, values, gate_cache, doc_ids,
    out_weight, mix_gain, gate_weight, up_weight, down_weight,
):
    group = REACH
    tok, all_cols = queries.shape
    features = residual.shape[1]
    heads_here = gate_cache.shape[1]
    head_size = all_cols // heads_here
    heads = heads_here // group
    rows = gate_cache.T.reshape(group, heads, tok)
    docs = jnp.broadcast_to(doc_ids.astype(jnp.float32), (group, 1, tok))
    fill = jnp.zeros((group, 7 - heads, tok), jnp.float32)
    aux = jnp.concatenate([rows, docs, fill], axis=1)
    cols, span, half = all_cols // group, tok * group, tok // 2
    width = gate_weight.shape[1] // group
    sources = 2 * planes
    sem = pltpu.SemaphoreType.DMA
    outside = pl.BlockSpec(memory_space=pltpu.HBM)
    inside = pl.BlockSpec(memory_space=pltpu.VMEM)
    bf16 = jnp.bfloat16
    four = sem((group,))
    return pl.pallas_call(
        functools.partial(layer_kernel, planes, head_size),
        out_shape=jax.ShapeDtypeStruct((half, features), bf16),
        in_specs=[outside] * 6 + [inside] + [outside] * 3,
        out_specs=inside,
        scratch_shapes=[
            pltpu.VMEM((span, cols), bf16),
            pltpu.VMEM((2 * span, cols), bf16),
            pltpu.VMEM((2 * span, cols), bf16),
            pltpu.VMEM((8, 2 * span), jnp.float32),
            pltpu.VMEM((span, cols), bf16),
            pltpu.VMEM((tok, all_cols), bf16),
            pltpu.VMEM(out_weight.shape, bf16),
            pltpu.VMEM((half, features), bf16),
            pltpu.VMEM((features, width), bf16),
            pltpu.VMEM((features, width), bf16),
            pltpu.VMEM((width, features), bf16),
            pltpu.VMEM((half, features), bf16),
            pltpu.VMEM((half, features), bf16),
            pltpu.VMEM((half, features), bf16),
            pltpu.VMEM((half, features), bf16),
            pltpu.VMEM((group, 2, half, features), bf16),
            pltpu.VMEM((group, tok, width), bf16),
            pltpu.VMEM((group, 2, half, features), bf16),
            pltpu.VMEM((group, half, features), bf16),
            pltpu.VMEM((group, half, features), bf16),
            pltpu.VMEM((group, half, features), bf16),
            sem((4, group)), sem((4, group)), sem((4,)),
            sem((3, group)), sem((3, group)),
            sem((3, sources)), sem((3, sources)), sem((3,)),
            sem((3, sources)), sem((3, sources)),
            four, four, sem, sem((2,)),
            sem, sem, four, four, four, four, four, four, four, four,
        ],
        compiler_params=pltpu.CompilerParams(
            collective_id=0, has_side_effects=True, vmem_limit_bytes=62 * 1024 * 1024
        ),
    )(
        residual, queries, keys, values, aux, out_weight, mix_gain.reshape(1, features),
        gate_weight, up_weight, down_weight,
    )


def choose(
    residual, queries, keys, values, gate_cache, doc_ids,
    out_weight, mix_gain, gate_weight, up_weight, down_weight,
):
    arrays = (
        residual, queries, keys, values, gate_cache, doc_ids,
        out_weight, mix_gain, gate_weight, up_weight, down_weight,
    )
    count, group = lax.axis_size("sp"), REACH
    planes = count // group
    heads = gate_cache.shape[1] // group
    fits = (
        count == planes * group
        and planes % 2 == 0
        and group == 4
        and lax.axis_size("tp") == 2
        and queries.shape[0] % 64 == 0
        and gate_cache.shape[1] == heads * group
        and 1 <= heads <= 7
        and queries.shape[0] % 128 == 0
        and (queries.shape[1] // group) % 128 == 0
        and gate_weight.shape[0] % 128 == 0
        and gate_weight.shape[1] % (group * 128) == 0
        and residual.shape[1] == gate_weight.shape[0] * count
        and residual.shape[1] % 512 == 0
        and queries.shape[0] * group >= 2 * planes * ROWS
    )
    return grouped_local(planes, *arrays) if fits else plain_local(*arrays)


def solution(mesh):
    return jax.shard_map(
        choose,
        mesh=mesh,
        in_specs=(
            P("sp", None),
            P("sp", "tp"),
            P("sp", "tp"),
            P("sp", "tp"),
            P("sp", "tp"),
            P("sp"),
            P("tp", None),
            P(),
            P("sp", "tp"),
            P("sp", "tp"),
            P("tp", "sp"),
        ),
        out_specs=P(("sp", "tp"), None),
        check_vma=False,
    )
```

time: 314 us -> 227 us (0.72)
  the two profiles are of different devices: /device:TPU:0 before, /device:TPU:5 now
where the time goes in v1:
time: 227 us
  Pallas kernels  223 us (98%)
  local copies, waits for them, and re-layouts  2.92 us (1%)
    pallas_call x1, Pallas kernels, grouped_local(): pl.pallas_call(functools.partial(layer_kernel, planes, head_size), out_sh...  223 us

profile of v1, /device:TPU:5, one launch (start us, length us, event | category | flops | bytes accessed | tf_op | source)
XLA Modules:
  0.0 227.2 jit_solution(10924106896197462469)
XLA Ops:
  0.0 0.1 pad.2.clone
  0.1 0.7 convert_element_type.3
  0.8 0.7 reshape.6
  1.5 0.7 maximum_maximum_fusion.aux
  2.2 222.9 %shard_map.109 = bf16[192,2048]{1,0:T(8,128)(2,1)} custom-call(bf16[384,2048]{1,0:T(8,128)(2,1)} %residual.1, bf16[384,1024]{1,0:T(8,128)(2,1)} %queries.1, bf16[384,1024]{1,0:T(8,128)(2,1)} %keys.1, bf16[384,1024]{1,0:T(8,128)(2,1)} %values.1, f32[4,8,384]{2,1,0:T(8,128)} %maximum_maximum_fusion.aux, bf16[1024,2048]{1,0:T(8,128)(2,1)} %out_weight.1, ...), custom_call_target="tpu_custom_call" | custom-call | tf_op jit(solution)/shard_map/pallas_call | solution.py:572
  225.1 2.1 copy.13
  (2 shorter events, 0.0 us)

commit v2 on v1

--- a/solution.py
+++ b/solution.py
@@ -277,22 +277,22 @@
         for m in range(3)
     ]
 
-    def pass_on(m, k):
-        its_plane, dx = planes - 1 - k // 2, lax.rem(k, 2)
-        e = lax.rem(plane - its_plane + planes, planes) * 2 + dx
-
-        @pl.when(e != 0)
-        def _():
-            held = slot(m, same_y(its_plane, lax.rem(x + dx, 2)))
+    arrivals = []
+    for p in range(planes):
+        over, under = range(p + 1, planes), range(p - 1, -1, -1)
+        order = [(z, 0) for z in over] + [(p, 1)] + [(z, 1) for z in over]
+        order += [(z, 0) for z in under] + [(z, 1) for z in under]
+        arrivals.append([(p - z) % planes * 2 + dx for z, dx in order])
+
+    def pass_on(m, i):
+        e = arrivals[-1][i]
+        for p in range(planes - 1):
+            e = jnp.where(plane == p, arrivals[p][i], e)
+        its_plane = lax.rem(plane - e // 2 + planes, planes)
+        held = slot(m, same_y(its_plane, lax.rem(x + lax.rem(e, 2), 2)))
+        with jax.named_scope(f"pass_{m}_{i}"):
             remote(held, held, w_send.at[m, e], w_recv.at[m, e], y_neighbour).wait_recv()
             remote(held, held, g_send.at[m, e], g_recv.at[m, e], y_neighbour).start()
-
-    def pass_range(m, first, last):
-        def one(k, carry):
-            pass_on(m, k)
-            return carry
-
-        lax.fori_loop(first, last, one, 0)
 
     def gathered(m):
         def one(e, carry):
@@ -344,8 +344,15 @@
 
     for m in range(3):
         forward_own[m].start()
-        for e in range(1, sources):
+        for e in range(2, sources, 2):
             pl.when(jnp.logical_not(upward(e)))(weights[m, e].start)
+
+    def issue(m, going_up):
+        for e in list(range(2, sources, 2)) + list(range(3, sources, 2)):
+            if going_up:
+                pl.when(upward(e))(weights[m, e].start)
+            elif e % 2:
+                pl.when(jnp.logical_not(upward(e)))(weights[m, e].start)
 
     @pl.when(plane == 0)
     def _():
@@ -353,18 +360,21 @@
         v_buf[pl.ds(0, span), :] = jnp.zeros((span, cols), jnp.bfloat16)
         aux_buf[:, pl.ds(0, span)] = jnp.zeros((aux_buf.shape[0], span), jnp.float32)
 
-    for step in range(1, group):
-        for copy in first_kinds[step]:
-            copy.wait_recv()
-
-        @pl.when(has_above)
+    for at_y, steps in ((0, (2, 3, 1)), (1, (1, 2, 3))):
+        @pl.when(y == at_y)
         def _():
-            for copy in halos[step]:
-                copy.start()
-
-    for m in range(3):
-        for e in range(2, sources):
-            pl.when(upward(e))(weights[m, e].start)
+            for step in steps:
+                for copy in first_kinds[step]:
+                    copy.wait_recv()
+
+                @pl.when(has_above)
+                def _():
+                    for copy in halos[step]:
+                        copy.start()
+
+    weights[0, 1].start()
+    weights[1, 1].start()
+    issue(0, False)
     for step in range(1, group):
         for copy in query_kinds[step]:
             copy.wait_recv()
@@ -387,24 +397,39 @@
             copy.start() if start else copy.wait()
 
     tiles = tok // ROWS
-    skip = max(0, group * tiles - sources - 1)
+    plan = {2: (0, 0), 4: (1, 0)}
+    for k in range(3):
+        plan[group * tiles - 3 + k] = (0, 1 + k)
+
+    def second():
+        issue(1, True)
+        issue(1, False)
+        weights[2, 1].start()
+
+    def third():
+        pl.when(low == 1)(functools.partial(issue, 2, True))
+
+    steps_of = (
+        (jnp.where(core == 0, 1, 4), functools.partial(issue, 0, True)),
+        (jnp.where(core == 0, 5, 8), second),
+        (jnp.where(core == 0, 9, 10), third),
+    )
 
     def rows_of(i, carry):
         at = group - 1 - i
 
         @pl.when(has_below)
         def _():
-            halo_arrived(at)
+            with jax.named_scope("halo"):
+                halo_arrived(at)
 
         def one(j, inner):
             attend_tile(at * tiles + tiles - 1 - j, plane, span, head_size,
                         q_buf, k_buf, v_buf, aux_buf, out_buf)
-            k = i * tiles + j - skip
-
-            @pl.when(jnp.logical_and(k >= 0, k < sources))
-            def _():
-                pass_on(0, k)
-
+            for at_tile, (m, k) in plan.items():
+                pl.when(i * tiles + j == at_tile)(functools.partial(pass_on, m, k))
+            for at_tile, step in steps_of:
+                pl.when(i * tiles + j == at_tile)(step)
             return inner
 
         lax.fori_loop(0, tiles, one, 0)
@@ -412,7 +437,6 @@
         return carry
 
     lax.fori_loop(0, group, rows_of, 0)
-    pass_range(1, 0, planes)
     for step in range(1, group):
         its = attended.at[:, head_cols(turned(step))]
         remote(its, its, b_send.at[step], b_recv.at[step], in_plane(step)).wait_recv()
@@ -449,74 +473,139 @@
         return carry
 
     lax.fori_loop(0, half // chunk, middle_rows, 0)
-    mine = tokens.at[own_block, core]
-    far = {e: remote(mine, mine, f_send.at[e], f_recv.at[e], quad(e)) for e in range(1, group)}
-    for e in (3, 1, 2):
-        far[e].start()
+    part_rows = half // 2
+
+    def shared(e, h):
+        return tokens.at[block(e), core, pl.ds(h * part_rows, part_rows), :]
+
+    def far_copy(e, h):
+        if e < 3:
+            return remote(shared(0, h), shared(0, h), f_send.at[e, h], f_recv.at[e, h], quad(e))
+        held = shared(1 + h, h)
+        return remote(held, held, f_send.at[e, h], f_recv.at[e, h], quad(2 - h))
+
+    far = {(e, h): far_copy(e, h) for e in range(1, group) for h in range(2)}
+    for e, h in ((1, 0), (2, 1), (1, 1), (2, 0)):
+        far[e, h].start()
     near = {}
     for e in range(group):
         held = tokens.at[block(e), core]
         near[e] = remote(held, held, n_send.at[e], n_recv.at[e], partner)
     near[0].start()
-    pass_range(1, planes, sources)
+    for k in range(4, sources - 1):
+        pass_on(0, k)
+    pass_on(2, 0)
+    pass_on(1, 1)
+    for h in range(2):
+        far[1 + h, h].wait_recv()
+        far[3, h].start()
+    pl.when(low == 0)(functools.partial(issue, 2, True))
+    issue(2, False)
+    for k in range(2, sources - 1):
+        pass_on(1, k)
     for e in range(1, group):
-        far[e].wait_recv()
+        for h in range(2):
+            if (e, h) not in ((1, 0), (2, 1)):
+                far[e, h].wait_recv()
         near[e].start()
     for m in range(2):
         kept[m].wait()
         gathered(m)
-    each = sources // group
-
-    def gate_and_up(e, carry):
-        index = lax.rem(low + e // 2, 2) * 2 + lax.rem(x + lax.rem(e, 2), 2)
+
+    def gate_and_up(e):
+        index = block(e)
         theirs = tokens.at[index, other]
         remote(theirs, theirs, n_send.at[e], n_recv.at[e], partner).wait_recv()
         rows = tokens[index].reshape(2 * half, features)
         gate_proj = jnp.dot(rows, gate_all[...], preferred_element_type=jnp.float32)
         up_proj = jnp.dot(rows, up_all[...], preferred_element_type=jnp.float32)
         hidden[index] = (gate_proj / (1.0 + jnp.exp(-gate_proj)) * up_proj).astype(jnp.bfloat16)
-        pass_range(2, e * each, (e + 1) * each)
-        return carry
-
-    lax.fori_loop(0, group, gate_and_up, 0)
+
+    for e in range(group):
+        gate_and_up(e)
+        for k in range(1 + e, 2 + e):
+            pass_on(2, k)
+    for k in range(1 + group, sources - 1):
+        pass_on(2, k)
     kept[2].wait()
-    gathered(2)
-    order = (3, 1, 2, 0)
     pairs, sent = {}, {}
-
-    def give(e):
+    run = 2 * depth
+
+    def columns(phase, its_plane):
+        its_y = y if phase == 0 else 1 - y
+        return pl.ds(pl.multiple_of(its_plane * group * depth + its_y * run, 128), run)
+
+    def lower(phase, e):
         index = block(e)
-        pairs[e].wait_recv()
+        rows = hidden[index]
+        for p in range(planes):
+            lowered = jnp.dot(rows, down_all[:, columns(phase, p)], preferred_element_type=jnp.float32)
+            part[phase, index, :, :, p * run : (p + 1) * run] = (
+                lowered.astype(jnp.bfloat16).reshape(2, half, run)
+            )
+        copy = remote(part.at[phase, index, other], pair.at[phase, index],
+                      p_send.at[phase, e], p_recv.at[phase, e], partner)
+        copy.start()
+        pairs[phase, e] = copy
+
+    def landing(phase, e, h):
+        return inbox.at[phase, e, pl.ds(h * part_rows, part_rows), :]
+
+    def give(phase, e, h, extra=None):
+        index = block(e)
 
         def one(i, carry):
-            at = pl.ds(pl.multiple_of(i * chunk, chunk), chunk)
-            both = part[index, core, at, :].astype(jnp.float32) + pair[index, at, :].astype(jnp.float32)
-            sums[e, at, :] = both.astype(jnp.bfloat16)
+            local = pl.ds(pl.multiple_of(i * chunk, chunk), chunk)
+            at = pl.ds(pl.multiple_of(h * part_rows + i * chunk, chunk), chunk)
+            both = part[phase, index, core, at, :].astype(jnp.float32)
+            both = both + pair[phase, index, at, :].astype(jnp.float32)
+            if extra is not None:
+                both = both + extra[local, :].astype(jnp.float32)
+            sums[phase, e, at, :] = both.astype(jnp.bfloat16)
             return carry
 
-        lax.fori_loop(0, half // chunk, one, 0)
-        sent[e] = remote(sums.at[e], inbox.at[e], r_send.at[e], r_recv.at[e], quad(e))
-        sent[e].start()
-
-    for i, e in enumerate(order):
-        index = block(e)
-        lowered = jnp.dot(hidden[index], down_all[...], preferred_element_type=jnp.float32)
-        part[index] = lowered.astype(jnp.bfloat16).reshape(2, half, features)
-        pairs[e] = remote(part.at[index, other], pair.at[index], p_send.at[e], p_recv.at[e], partner)
-        pairs[e].start()
-        if i > 0:
-            give(order[i - 1])
-    pairs[0].wait_recv()
-    for e in range(1, group):
-        sent[e].wait_recv()
+        lax.fori_loop(0, part_rows // chunk, one, 0)
+        kind, to = (0, 1 + h) if e == 3 else (e, e)
+        copy = remote(sums.at[phase, e, pl.ds(h * part_rows, part_rows), :], landing(phase, kind, h),
+                      r_send.at[phase, kind, h], r_recv.at[phase, kind, h], quad(to))
+        copy.start()
+        sent[phase, e, h] = copy
+
+    for phase in range(2):
+        if phase:
+            gathered(2)
+        lower(phase, 3)
+        lower(phase, 1)
+        pairs[phase, 3].wait_recv()
+        give(phase, 3, 0)
+        give(phase, 3, 1)
+        lower(phase, 2)
+        pairs[phase, 1].wait_recv()
+        give(phase, 1, 0)
+        lower(phase, 0)
+        pairs[phase, 2].wait_recv()
+        give(phase, 2, 1)
+        sent[phase, 3, 1].wait_recv()
+        give(phase, 1, 1, landing(phase, 0, 1))
+        sent[phase, 3, 0].wait_recv()
+        give(phase, 2, 0, landing(phase, 0, 0))
+    for phase in range(2):
+        pairs[phase, 0].wait_recv()
+        for e in (1, 2):
+            for h in range(2):
+                sent[phase, e, h].wait_recv()
 
     def last_rows(i, carry):
         at = pl.ds(pl.multiple_of(i * chunk, chunk), chunk)
-        total = part[own_block, core, at, :].astype(jnp.float32)
-        total = total + pair[own_block, at, :].astype(jnp.float32)
-        for e in range(1, group):
-            total = total + inbox[e, at, :].astype(jnp.float32)
-        out[at, :] = (mid[at, :].astype(jnp.float32) + total).astype(jnp.bfloat16)
+        for phase in range(2):
+            for p in range(planes):
+                lanes = slice(p * run, (p + 1) * run)
+                total = part[phase, own_block, core, at, lanes].astype(jnp.float32)
+                total = total + pair[phase, own_block, at, lanes].astype(jnp.float32)
+                for e in range(1, group - 1):
+                    total = total + inbox[phase, e, at, lanes].astype(jnp.float32)
+                cols_at = columns(phase, p)
+                out[at, cols_at] = (mid[at, cols_at].astype(jnp.float32) + total).astype(jnp.bfloat16)
         return carry
 
     lax.fori_loop(0, half // chunk, last_rows, 0)
@@ -592,16 +681,17 @@
             pltpu.VMEM((half, features), bf16),
             pltpu.VMEM((group, 2, half, features), bf16),
             pltpu.VMEM((group, tok, width), bf16),
-            pltpu.VMEM((group, 2, half, features), bf16),
-            pltpu.VMEM((group, half, features), bf16),
-            pltpu.VMEM((group, half, features), bf16),
-            pltpu.VMEM((group, half, features), bf16),
+            pltpu.VMEM((2, group, 2, half, features // 2), bf16),
+            pltpu.VMEM((2, group, half, features // 2), bf16),
+            pltpu.VMEM((2, group, half, features // 2), bf16),
+            pltpu.VMEM((2, group - 1, half, features // 2), bf16),
             sem((4, group)), sem((4, group)), sem((4,)),
             sem((3, group)), sem((3, group)),
             sem((3, sources)), sem((3, sources)), sem((3,)),
             sem((3, sources)), sem((3, sources)),
             four, four, sem, sem((2,)),
-            sem, sem, four, four, four, four, four, four, four, four,
+            sem, sem, four, four, sem((group, 2)), sem((group, 2)),
+            sem((2, group)), sem((2, group)), sem((2, 3, 2)), sem((2, 3, 2)),
         ],
         compiler_params=pltpu.CompilerParams(
             collective_id=0, has_side_effects=True, vmem_limit_bytes=62 * 1024 * 1024
@@ -626,6 +716,7 @@
     fits = (
         count == planes * group
         and planes % 2 == 0
+        and planes == group
         and group == 4
         and lax.axis_size("tp") == 2
         and queries.shape[0] % 64 == 0

time: 227 us -> 187 us (0.82)
  the two profiles are of different devices: /device:TPU:5 before, /device:TPU:21 now
where the time goes in v2:
time: 187 us; the launch traced here: 186 us
  Pallas kernels  182 us (97%)
  local copies, waits for them, and re-layouts  2.92 us (2%)
    pallas_call x1, Pallas kernels, grouped_local(): pl.pallas_call(functools.partial(layer_kernel, planes, head_size), out_sh...  182 us

profile of v2, /device:TPU:21, one launch (start us, length us, event | category | flops | bytes accessed | tf_op | source)
XLA Modules:
  0.0 186.5 jit_solution(5634478375838003043)
XLA Ops:
  0.0 0.1 pad.2.clone
  0.1 0.7 convert_element_type.3
  0.8 0.7 reshape.6
  1.5 0.7 maximum_maximum_fusion.aux
  2.2 182.2 %shard_map.109 = bf16[192,2048]{1,0:T(8,128)(2,1)} custom-call(bf16[384,2048]{1,0:T(8,128)(2,1)} %residual.1, bf16[384,1024]{1,0:T(8,128)(2,1)} %queries.1, bf16[384,1024]{1,0:T(8,128)(2,1)} %keys.1, bf16[384,1024]{1,0:T(8,128)(2,1)} %values.1, f32[4,8,384]{2,1,0:T(8,128)} %maximum_maximum_fusion.aux, bf16[1024,2048]{1,0:T(8,128)(2,1)} %out_weight.1, ...), custom_call_target="tpu_custom_call" | custom-call | tf_op jit(solution)/shard_map/pallas_call | solution.py:661
  184.4 2.1 %copy.13 = bf16[192,2048]{1,0:T(8,128)(2,1)} copy(bf16[192,2048]{1,0:T(8,128)(2,1)} %shard_map.109) | data formatting | bytes 1572864
  (2 shorter events, 0.0 us)

commit v3 on v2

--- a/solution.py
+++ b/solution.py
@@ -146,9 +146,9 @@
 
 def layer_kernel(
     planes, head_size,
-    residual, queries, keys, values, aux, out_weight, gain, gate, up, down,
+    residual, queries, keys, values, cache, docs, out_weight, gain, gate, up, down,
     out,
-    q_buf, k_buf, v_buf, aux_buf, out_buf, attended, out_w, res_buf,
+    aux, q_buf, k_buf, v_buf, aux_buf, out_buf, attended, out_w, res_buf,
     gate_all, up_all, down_all, theirs_buf, mine_buf, got, mid, tokens, hidden,
     part, pair, sums, inbox,
     a_send, a_recv, a_own, h_send, h_recv, w_send, w_recv, w_own, g_send, g_recv,
@@ -203,6 +203,12 @@
     def greet(device):
         pl.semaphore_signal(barrier, inc=1, device_id=device, device_id_type=MESH)
 
+    heads = cache.shape[0] // group
+    numbers = docs[...].astype(jnp.float32).reshape(1, tok)
+    for index in range(group):
+        aux[index, 0:heads, :] = cache[index * heads : (index + 1) * heads, :]
+        aux[index, heads : heads + 1, :] = numbers
+        aux[index, heads + 1 :, :] = jnp.zeros((aux.shape[1] - heads - 1, tok), jnp.float32)
     greet(partner)
     for step in range(2, group):
         greet(in_plane(step))
@@ -279,8 +285,11 @@
 
     arrivals = []
     for p in range(planes):
-        over, under = range(p + 1, planes), range(p - 1, -1, -1)
-        order = [(z, 0) for z in over] + [(p, 1)] + [(z, 1) for z in over]
+        mate = p ^ 1
+        over = [z for z in range(p + 1, planes) if z != mate]
+        under = [z for z in range(p - 1, -1, -1) if z != mate]
+        order = [(mate, 0), (p, 1)] if mate > p else [(p, 1), (mate, 0)]
+        order += [(mate, 1)] + [(z, 0) for z in over] + [(z, 1) for z in over]
         order += [(z, 0) for z in under] + [(z, 1) for z in under]
         arrivals.append([(p - z) % planes * 2 + dx for z, dx in order])
 
@@ -294,15 +303,15 @@
             remote(held, held, w_send.at[m, e], w_recv.at[m, e], y_neighbour).wait_recv()
             remote(held, held, g_send.at[m, e], g_recv.at[m, e], y_neighbour).start()
 
-    def gathered(m):
-        def one(e, carry):
-            its_plane = lax.rem(plane - e // 2 + planes, planes)
-            its_x = lax.rem(x + lax.rem(e, 2), 2)
-            held = slot(m, its_plane * group + 2 * (1 - y) + its_x)
+    def gathered(m, its_high):
+        def one(k, carry):
+            its_plane, dx = its_high * 2 + k // 2, lax.rem(k, 2)
+            e = lax.rem(plane - its_plane + planes, planes) * 2 + dx
+            held = slot(m, its_plane * group + 2 * (1 - y) + lax.rem(x + dx, 2))
             remote(held, held, g_send.at[m, e], g_recv.at[m, e], y_neighbour).wait_recv()
             return carry
 
-        lax.fori_loop(0, sources, one, 0)
+        lax.fori_loop(0, 4, one, 0)
 
     own = [
         pltpu.make_async_copy(keys.at[:, head_cols(place)], k_buf.at[late(place), :], a_own.at[0]),
@@ -320,39 +329,39 @@
     ]
     has_above, has_below = plane < planes - 1, plane > 0
 
+    far_first = (3, 1, 2)
     first_kinds = {step: spread(step, (0, 1, 2)) for step in range(1, group)}
     query_kinds = {step: spread(step, (3,)) for step in range(1, group)}
     halos = {step: halo(step) for step in range(group)}
-    for step in range(1, group):
+    weights = {(m, e): weight(m, e) for m in range(3) for e in range(1, sources)}
+
+    def upward(e):
+        return jnp.logical_and(e // 2 > 0, plane + e // 2 < planes)
+
+    for step in far_first:
         for copy in first_kinds[step]:
             copy.start()
-
-    @pl.when(has_above)
-    def _():
-        for copy in halos[0]:
-            copy.start()
-
-    for step in range(1, group):
+    filling = (2, 4)
+    for e in filling:
+        pl.when(upward(e))(weights[0, e].start)
+    for step in far_first:
         for copy in query_kinds[step]:
             copy.start()
     for copy in own + kept + loads:
         copy.start()
-    weights = {(m, e): weight(m, e) for m in range(3) for e in range(1, sources)}
-
-    def upward(e):
-        return jnp.logical_and(e // 2 > 0, plane + e // 2 < planes)
-
     for m in range(3):
         forward_own[m].start()
         for e in range(2, sources, 2):
             pl.when(jnp.logical_not(upward(e)))(weights[m, e].start)
 
-    def issue(m, going_up):
-        for e in list(range(2, sources, 2)) + list(range(3, sources, 2)):
-            if going_up:
+    def issue_up(m, first_e):
+        for e in range(first_e, sources, 2):
+            if m > 0 or e not in filling:
                 pl.when(upward(e))(weights[m, e].start)
-            elif e % 2:
-                pl.when(jnp.logical_not(upward(e)))(weights[m, e].start)
+
+    def issue_down(m):
+        for e in range(3, sources, 2):
+            pl.when(jnp.logical_not(upward(e)))(weights[m, e].start)
 
     @pl.when(plane == 0)
     def _():
@@ -360,24 +369,20 @@
         v_buf[pl.ds(0, span), :] = jnp.zeros((span, cols), jnp.bfloat16)
         aux_buf[:, pl.ds(0, span)] = jnp.zeros((aux_buf.shape[0], span), jnp.float32)
 
-    for at_y, steps in ((0, (2, 3, 1)), (1, (1, 2, 3))):
-        @pl.when(y == at_y)
+    for its_place in range(group):
+        @pl.when(place == its_place)
         def _():
-            for step in steps:
-                for copy in first_kinds[step]:
-                    copy.wait_recv()
+            for at in range(group - 1, -1, -1):
+                step = its_place ^ at
+                if step:
+                    for copy in first_kinds[step]:
+                        copy.wait_recv()
 
                 @pl.when(has_above)
                 def _():
                     for copy in halos[step]:
                         copy.start()
 
-    weights[0, 1].start()
-    weights[1, 1].start()
-    issue(0, False)
-    for step in range(1, group):
-        for copy in query_kinds[step]:
-            copy.wait_recv()
     for copy in own:
         copy.wait()
 
@@ -397,26 +402,44 @@
             copy.start() if start else copy.wait()
 
     tiles = tok // ROWS
-    plan = {2: (0, 0), 4: (1, 0)}
-    for k in range(3):
-        plan[group * tiles - 3 + k] = (0, 1 + k)
+    last_tile = group * tiles - 1
+    plan = {5: (0, 0), 6: (1, 0), last_tile - 4: (0, 1), last_tile - 2: (0, 2), last_tile: (0, 3)}
+
+    def first():
+        weights[0, 1].start()
+        weights[1, 1].start()
+        issue_down(0)
 
     def second():
-        issue(1, True)
-        issue(1, False)
+        issue_up(0, 2)
+        issue_up(0, 3)
+
+    def third():
+        issue_up(1, 2)
+        issue_up(1, 3)
+        issue_down(1)
         weights[2, 1].start()
 
-    def third():
-        pl.when(low == 1)(functools.partial(issue, 2, True))
+    def fourth():
+        for e in range(2, sources):
+            pl.when(jnp.logical_and(low == 1, upward(e)))(weights[2, e].start)
 
     steps_of = (
-        (jnp.where(core == 0, 1, 4), functools.partial(issue, 0, True)),
-        (jnp.where(core == 0, 5, 8), second),
-        (jnp.where(core == 0, 9, 10), third),
+        (jnp.where(core == 0, 3, 4), first),
+        (jnp.where(core == 0, 4, 6), second),
+        (jnp.where(core == 0, 6, 7), third),
+        (jnp.where(core == 0, last_tile - 1, last_tile), fourth),
     )
 
     def rows_of(i, carry):
         at = group - 1 - i
+
+        @pl.when(at != place)
+        def _():
+            rows = q_buf.at[early(at), :]
+            step = lax.rem(x + lax.rem(at, 2), 2) + 2 * lax.rem(y + at // 2, 2)
+            with jax.named_scope("queries"):
+                remote(rows, rows, a_send.at[3, step], a_recv.at[3, step], below).wait_recv()
 
         @pl.when(has_below)
         def _():
@@ -499,18 +522,15 @@
     for h in range(2):
         far[1 + h, h].wait_recv()
         far[3, h].start()
-    pl.when(low == 0)(functools.partial(issue, 2, True))
-    issue(2, False)
+    for e in range(2, sources):
+        pl.when(jnp.logical_and(low == 0, upward(e)))(weights[2, e].start)
+    issue_down(2)
     for k in range(2, sources - 1):
         pass_on(1, k)
-    for e in range(1, group):
-        for h in range(2):
-            if (e, h) not in ((1, 0), (2, 1)):
-                far[e, h].wait_recv()
-        near[e].start()
     for m in range(2):
         kept[m].wait()
-        gathered(m)
+        gathered(m, 0)
+        gathered(m, 1)
 
     def gate_and_up(e):
         index = block(e)
@@ -521,24 +541,32 @@
         up_proj = jnp.dot(rows, up_all[...], preferred_element_type=jnp.float32)
         hidden[index] = (gate_proj / (1.0 + jnp.exp(-gate_proj)) * up_proj).astype(jnp.bfloat16)
 
-    for e in range(group):
-        gate_and_up(e)
-        for k in range(1 + e, 2 + e):
-            pass_on(2, k)
-    for k in range(1 + group, sources - 1):
-        pass_on(2, k)
+    for e in range(1, group):
+        with jax.named_scope(f"far{e}"):
+            for h in range(2):
+                if (e, h) not in ((1, 0), (2, 1)):
+                    far[e, h].wait_recv()
+        near[e].start()
+        gate_and_up(e - 1)
+        for k in range(1, e):
+            if e > 1:
+                pass_on(2, 1 if e == 2 else 1 + k)
+    gate_and_up(group - 1)
+    pass_on(2, group)
     kept[2].wait()
     pairs, sent = {}, {}
     run = 2 * depth
-
-    def columns(phase, its_plane):
-        its_y = y if phase == 0 else 1 - y
-        return pl.ds(pl.multiple_of(its_plane * group * depth + its_y * run, 128), run)
+    phases = 4
+
+    def columns(phase, p):
+        its_y = y if phase < 2 else 1 - y
+        its_high = high if phase % 2 == 0 else 1 - high
+        return pl.ds(pl.multiple_of(((its_high * 2 + p) * group + 2 * its_y) * depth, 128), run)
 
     def lower(phase, e):
         index = block(e)
         rows = hidden[index]
-        for p in range(planes):
+        for p in range(2):
             lowered = jnp.dot(rows, down_all[:, columns(phase, p)], preferred_element_type=jnp.float32)
             part[phase, index, :, :, p * run : (p + 1) * run] = (
                 lowered.astype(jnp.bfloat16).reshape(2, half, run)
@@ -571,25 +599,28 @@
         copy.start()
         sent[phase, e, h] = copy
 
-    for phase in range(2):
-        if phase:
-            gathered(2)
-        lower(phase, 3)
-        lower(phase, 1)
-        pairs[phase, 3].wait_recv()
-        give(phase, 3, 0)
-        give(phase, 3, 1)
-        lower(phase, 2)
-        pairs[phase, 1].wait_recv()
-        give(phase, 1, 0)
-        lower(phase, 0)
-        pairs[phase, 2].wait_recv()
-        give(phase, 2, 1)
+    def combine(phase):
         sent[phase, 3, 1].wait_recv()
         give(phase, 1, 1, landing(phase, 0, 1))
         sent[phase, 3, 0].wait_recv()
         give(phase, 2, 0, landing(phase, 0, 0))
-    for phase in range(2):
+
+    for phase in range(phases):
+        if phase == 1:
+            for k in range(1 + group, sources - 1):
+                pass_on(2, k)
+        if phase > 1:
+            gathered(2, high if phase == 2 else 1 - high)
+        for e in (3, 1, 2, 0):
+            lower(phase, e)
+        if phase:
+            combine(phase - 1)
+        for e, h in ((3, 0), (3, 1), (1, 0), (2, 1)):
+            if h == 0 or e == 2:
+                pairs[phase, e].wait_recv()
+            give(phase, e, h)
+    combine(phases - 1)
+    for phase in range(phases):
         pairs[phase, 0].wait_recv()
         for e in (1, 2):
             for h in range(2):
@@ -597,8 +628,8 @@
 
     def last_rows(i, carry):
         at = pl.ds(pl.multiple_of(i * chunk, chunk), chunk)
-        for phase in range(2):
-            for p in range(planes):
+        for phase in range(phases):
+            for p in range(2):
                 lanes = slice(p * run, (p + 1) * run)
                 total = part[phase, own_block, core, at, lanes].astype(jnp.float32)
                 total = total + pair[phase, own_block, at, lanes].astype(jnp.float32)
@@ -645,11 +676,6 @@
     features = residual.shape[1]
     heads_here = gate_cache.shape[1]
     head_size = all_cols // heads_here
-    heads = heads_here // group
-    rows = gate_cache.T.reshape(group, heads, tok)
-    docs = jnp.broadcast_to(doc_ids.astype(jnp.float32), (group, 1, tok))
-    fill = jnp.zeros((group, 7 - heads, tok), jnp.float32)
-    aux = jnp.concatenate([rows, docs, fill], axis=1)
     cols, span, half = all_cols // group, tok * group, tok // 2
     width = gate_weight.shape[1] // group
     sources = 2 * planes
@@ -661,9 +687,10 @@
     return pl.pallas_call(
         functools.partial(layer_kernel, planes, head_size),
         out_shape=jax.ShapeDtypeStruct((half, features), bf16),
-        in_specs=[outside] * 6 + [inside] + [outside] * 3,
+        in_specs=[outside] * 4 + [inside] * 2 + [outside, inside] + [outside] * 3,
         out_specs=inside,
         scratch_shapes=[
+            pltpu.VMEM((group, 8, tok), jnp.float32),
             pltpu.VMEM((span, cols), bf16),
             pltpu.VMEM((2 * span, cols), bf16),
             pltpu.VMEM((2 * span, cols), bf16),
@@ -681,23 +708,24 @@
             pltpu.VMEM((half, features), bf16),
             pltpu.VMEM((group, 2, half, features), bf16),
             pltpu.VMEM((group, tok, width), bf16),
-            pltpu.VMEM((2, group, 2, half, features // 2), bf16),
-            pltpu.VMEM((2, group, half, features // 2), bf16),
-            pltpu.VMEM((2, group, half, features // 2), bf16),
-            pltpu.VMEM((2, group - 1, half, features // 2), bf16),
+            pltpu.VMEM((4, group, 2, half, features // 4), bf16),
+            pltpu.VMEM((4, group, half, features // 4), bf16),
+            pltpu.VMEM((4, group, half, features // 4), bf16),
+            pltpu.VMEM((4, group - 1, half, features // 4), bf16),
             sem((4, group)), sem((4, group)), sem((4,)),
             sem((3, group)), sem((3, group)),
             sem((3, sources)), sem((3, sources)), sem((3,)),
             sem((3, sources)), sem((3, sources)),
             four, four, sem, sem((2,)),
             sem, sem, four, four, sem((group, 2)), sem((group, 2)),
-            sem((2, group)), sem((2, group)), sem((2, 3, 2)), sem((2, 3, 2)),
+            sem((4, group)), sem((4, group)), sem((4, 3, 2)), sem((4, 3, 2)),
         ],
         compiler_params=pltpu.CompilerParams(
             collective_id=0, has_side_effects=True, vmem_limit_bytes=62 * 1024 * 1024
         ),
     )(
-        residual, queries, keys, values, aux, out_weight, mix_gain.reshape(1, features),
+        residual, queries, keys, values, gate_cache.T, doc_ids, out_weight,
+        mix_gain.reshape(1, features),
         gate_weight, up_weight, down_weight,
     )
 
@@ -721,7 +749,7 @@
         and lax.axis_size("tp") == 2
         and queries.shape[0] % 64 == 0
         and gate_cache.shape[1] == heads * group
-        and 1 <= heads <= 7
+        and 1 <= heads <= 6
         and queries.shape[0] % 128 == 0
         and (queries.shape[1] // group) % 128 == 0
         and gate_weight.shape[0] % 128 == 0

time: 187 us -> 180 us (0.963)
  the two profiles are of different devices: /device:TPU:21 before, /device:TPU:0 now
where the time goes in v3:
time: 180 us
  Pallas kernels  178 us (99%)
  local copies, waits for them, and re-layouts  2.09 us (1%)
    pallas_call x1, Pallas kernels, grouped_local(): pl.pallas_call(functools.partial(layer_kernel, planes, head_size), out_sh...  178 us

profile of v3, /device:TPU:0, one launch (start us, length us, event | category | flops | bytes accessed | tf_op | source)
XLA Modules:
  0.0 179.8 jit_solution(5460909271848620797)
XLA Ops:
  0.0 177.7 %shard_map.109 = bf16[192,2048]{1,0:T(8,128)(2,1)} custom-call(bf16[384,2048]{1,0:T(8,128)(2,1)} %residual.1, bf16[384,1024]{1,0:T(8,128)(2,1)} %queries.1, bf16[384,1024]{1,0:T(8,128)(2,1)} %keys.1, bf16[384,1024]{1,0:T(8,128)(2,1)} %values.1, f32[16,384]{1,0:T(8,128)} %bitcast.2, s32[384]{0:T(512)} %docs.1, bf16[1024,2048]{1,0:T(8,128)(2,1)} %out_weight.1, ...), custom_call_target="tpu_custom_call" | custom-call | tf_op jit(solution)/shard_map/pallas_call | solution.py:687
  177.7 2.1 %copy.13 = bf16[192,2048]{1,0:T(8,128)(2,1)} copy(bf16[192,2048]{1,0:T(8,128)(2,1)} %shard_map.109) | data formatting | bytes 1572864

commit v4 on v3

--- a/solution.py
+++ b/solution.py
@@ -417,7 +417,6 @@
     def third():
         issue_up(1, 2)
         issue_up(1, 3)
-        issue_down(1)
         weights[2, 1].start()
 
     def fourth():
@@ -427,7 +426,7 @@
     steps_of = (
         (jnp.where(core == 0, 3, 4), first),
         (jnp.where(core == 0, 4, 6), second),
-        (jnp.where(core == 0, 6, 7), third),
+        (jnp.where(core == 0, 5, 6), third),
         (jnp.where(core == 0, last_tile - 1, last_tile), fourth),
     )
 
@@ -460,6 +459,7 @@
         return carry
 
     lax.fori_loop(0, group, rows_of, 0)
+    issue_down(1)
     for step in range(1, group):
         its = attended.at[:, head_cols(turned(step))]
         remote(its, its, b_send.at[step], b_recv.at[step], in_plane(step)).wait_recv()
@@ -518,14 +518,15 @@
     for k in range(4, sources - 1):
         pass_on(0, k)
     pass_on(2, 0)
-    pass_on(1, 1)
+    for k in range(1, 5):
+        pass_on(1, k)
     for h in range(2):
         far[1 + h, h].wait_recv()
         far[3, h].start()
     for e in range(2, sources):
         pl.when(jnp.logical_and(low == 0, upward(e)))(weights[2, e].start)
     issue_down(2)
-    for k in range(2, sources - 1):
+    for k in range(5, sources - 1):
         pass_on(1, k)
     for m in range(2):
         kept[m].wait()

time: 180 us -> 178 us (0.989)
  Pallas kernels: 178 us -> 175 us
    pallas_call x1, Pallas kernels: 178 us -> 175 us  [grouped_local(): pl.pallas_call(functools.partial(layer_kernel, planes, head_size), out_sh...]
where the time goes in v4:
time: 178 us; the launch traced here: 177 us
  Pallas kernels  175 us (98%)
  local copies, waits for them, and re-layouts  2.09 us (1%)
    pallas_call x1, Pallas kernels, grouped_local(): pl.pallas_call(functools.partial(layer_kernel, planes, head_size), out_sh...  175 us

profile of v4, /device:TPU:0, one launch (start us, length us, event | category | flops | bytes accessed | tf_op | source)
XLA Modules:
  0.0 176.9 jit_solution(6246513135275141695)
XLA Ops:
  0.0 174.8 %shard_map.109 = bf16[192,2048]{1,0:T(8,128)(2,1)} custom-call(bf16[384,2048]{1,0:T(8,128)(2,1)} %residual.1, bf16[384,1024]{1,0:T(8,128)(2,1)} %queries.1, bf16[384,1024]{1,0:T(8,128)(2,1)} %keys.1, bf16[384,1024]{1,0:T(8,128)(2,1)} %values.1, f32[16,384]{1,0:T(8,128)} %bitcast.2, s32[384]{0:T(512)} %docs.1, bf16[1024,2048]{1,0:T(8,128)(2,1)} %out_weight.1, ...), custom_call_target="tpu_custom_call" | custom-call | tf_op jit(solution)/shard_map/pallas_call | solution.py:688
  174.8 2.1 %copy.13 = bf16[192,2048]{1,0:T(8,128)(2,1)} copy(bf16[192,2048]{1,0:T(8,128)(2,1)} %shard_map.109) | data formatting | bytes 1572864
